TPU v7x, 256 devices: a whole 4x4x8 slice. The times are simulated.
256 devices in a mesh: ep: 64 (over z, x, core), tp: 4 (over y).
Axes of the slice: x: 4, y: 4, z: 8, core: 2. Of those that a mesh axis runs over, the one named last changes fastest.
Arguments:
- queries: bfloat16 [16384, 1024], P('ep', 'tp'), may hold values from -6 to 6
- keys: bfloat16 [16384, 256], P('ep', 'tp'), may hold values from -6 to 6
- values: bfloat16 [16384, 256], P('ep', 'tp'), may hold values from -6 to 6
- q_gain: float32 [64], replicated, may hold values from 1 to 6
- k_gain: float32 [64], replicated, may hold values from 1 to 6
- out_weight: bfloat16 [1024, 2048], P('tp'), may hold values from -0.1875 to 0.1875
- tokens: bfloat16 [8192, 2048], P(('ep', 'tp')), may hold values from -6 to 6
- ffn_gain: float32 [2048], replicated, may hold values from 0.1 to 1.9
- route: int32 [8192, 2], P(('ep', 'tp')), may hold values from 0 to 63, all different within a row; in each aligned block of 32 rows (0 to 31, 32 to 63, ...) at most 2 rows name the same one
- route_weight: float32 [8192, 2], P(('ep', 'tp')), may hold values from 0.1 to 1
- gate_weight: bfloat16 [64, 2048, 3584], P('ep', None, 'tp'), may hold values from -0.125 to 0.125
- up_weight: bfloat16 [64, 2048, 3584], P('ep', None, 'tp'), may hold values from -0.125 to 0.125
- down_weight: bfloat16 [64, 3584, 2048], P('ep', 'tp'), may hold values from -0.09375 to 0.09375
Outputs:
- mixer_out: bfloat16 [16384, 2048], P(('ep', 'tp'))
- mixed: bfloat16 [8192, 2048], P(('ep', 'tp'))
Inputs may be any that keep to these rules, and one draw needn't show every extreme that they name: `route`: each row names 2 different experts. In every device's aligned block of 32 rows no expert is named more than 2 times, and in some blocks some expert is named exactly 2 times.
All inputs are finite; a program needn't handle non-finite values.
Results may differ from a plain program's by a relative error of at most 0.013.
The roundings to bfloat16 on the way count: a program that leaves them out, or rounds other values in their place, can miss the bound.
Values may be sent and summed in bfloat16 or wider, within the bound.
A program may use at most 192 MiB of HBM per device.

v0:
```python
import jax
import jax.numpy as jnp
from jax import lax
from jax.sharding import PartitionSpec as P

GRID_W = 64


EPS = 1e-06
THETA = 10000.0


def laid_out(blocks, dim):
    shape = list(blocks.shape[1:])
    shape[dim] *= blocks.shape[0]
    return jnp.moveaxis(blocks, 0, dim).reshape(shape)


def copy_for_each(array, axis):
    copies = jnp.broadcast_to(array, (lax.axis_size(axis), *array.shape))
    return lax.all_to_all(copies, axis, split_axis=0, concat_axis=0, tiled=True)


def collect(array, axis, dim):
    return laid_out(copy_for_each(array, axis), dim)


def in_blocks(array, dim, peers):
    before, after = (array.shape[:dim], array.shape[dim + 1 :])
    return jnp.moveaxis(array.reshape(*before, peers, -1, *after), dim, 0)


def sum_at_owner(array, axis, dim):
    blocks = in_blocks(array, dim, lax.axis_size(axis))
    arrived = lax.all_to_all(blocks, axis, split_axis=0, concat_axis=0, tiled=True)
    return arrived.astype(jnp.float32).sum(axis=0)


def head_norm(vals, gain):
    vals = vals.astype(jnp.float32)
    return vals * lax.rsqrt(jnp.mean(vals * vals, axis=-1, keepdims=True) + EPS) * gain


def rotate(vals, positions):
    pairs = vals.shape[-1] // 2
    quarter = pairs // 2
    freqs = THETA ** (-jnp.arange(quarter, dtype=jnp.float32) / quarter)
    grid_row = (positions // GRID_W).astype(jnp.float32)
    grid_col = (positions % GRID_W).astype(jnp.float32)
    angle = jnp.concatenate([grid_row[:, None] * freqs, grid_col[:, None] * freqs], axis=-1)
    cosine = jnp.cos(angle)[:, None, :]
    sine = jnp.sin(angle)[:, None, :]
    split = vals.reshape(vals.shape[:-1] + (pairs, 2))
    first = split[..., 0]
    second = split[..., 1]
    turned = jnp.stack([first * cosine - second * sine, first * sine + second * cosine], axis=-1)
    return turned.reshape(vals.shape)


def local(
    queries,
    keys,
    values,
    q_gain,
    k_gain,
    out_weight,
    tokens,
    ffn_gain,
    route,
    route_weight,
    gate_weight,
    up_weight,
    down_weight,
):
    local_rows = queries.shape[0]
    head_size = q_gain.shape[0]
    query_heads = queries.shape[1] // head_size
    key_heads = keys.shape[1] // head_size
    group = query_heads // key_heads
    key_width = key_heads * head_size
    positions = lax.axis_index("ep") * local_rows + jnp.arange(local_rows, dtype=jnp.int32)
    rot_q = rotate(
        head_norm(queries.reshape(local_rows, query_heads, head_size), q_gain), positions
    ).astype(jnp.bfloat16)
    rot_q = rot_q.reshape(local_rows, key_heads, group, head_size)
    rot_k = rotate(
        head_norm(keys.reshape(local_rows, key_heads, head_size), k_gain), positions
    ).astype(jnp.bfloat16)
    joined = jnp.concatenate([rot_k.reshape(local_rows, key_width), values], axis=1)
    scale = head_size ** (-0.5)

    def fold_block(carry, block):
        highest, denom, numer = carry
        key_block = block[:, :key_width].reshape(-1, key_heads, head_size)
        value_block = block[:, key_width:].reshape(-1, key_heads, head_size)
        scores = (
            jnp.einsum("qkgd,skd->qkgs", rot_q, key_block, preferred_element_type=jnp.float32)
            * scale
        )
        new_high = jnp.maximum(highest, jnp.max(scores, axis=-1))
        shrink = jnp.exp(highest - new_high)
        expo = jnp.exp(scores - new_high[..., None])
        denom = denom * shrink + jnp.sum(expo, axis=-1)
        numer = numer * shrink[..., None] + jnp.einsum(
            "qkgs,skd->qkgd",
            expo.astype(jnp.bfloat16),
            value_block,
            preferred_element_type=jnp.float32,
        )
        return ((new_high, denom, numer), None)

    start_high = jnp.full((local_rows, key_heads, group), -1e30, jnp.float32)
    start_denom = jnp.zeros((local_rows, key_heads, group), jnp.float32)
    start_numer = jnp.zeros((local_rows, key_heads, group, head_size), jnp.float32)
    carry = (start_high, start_denom, start_numer)
    piece = lax.all_gather(joined, "ep", axis=0, tiled=True)
    length = piece.shape[0]
    size = length
    while size > 2048 and size % 2 == 0:
        size = size // 2
    blocks = piece.reshape(length // size, size, piece.shape[1])
    carry, _ = lax.scan(fold_block, carry, blocks)
    highest, denom, numer = carry
    attended = (
        (numer / denom[..., None]).astype(jnp.bfloat16).reshape(local_rows, query_heads * head_size)
    )
    own_rows = tokens.shape[0]
    width = tokens.shape[1]
    picks_row = route.shape[1]
    experts = lax.axis_size("ep")
    capacity = 2 * own_rows * picks_row // experts
    token_float = tokens.astype(jnp.float32)
    normed = (
        token_float
        * lax.rsqrt(jnp.mean(token_float * token_float, axis=-1, keepdims=True) + EPS)
        * ffn_gain
    ).astype(jnp.bfloat16)
    flat_route = route.reshape(-1)
    expert_hot = (flat_route[:, None] == jnp.arange(experts, dtype=jnp.int32)[None, :]).astype(
        jnp.int32
    )
    earlier = jnp.cumsum(expert_hot, axis=0) - expert_hot
    rank = jnp.sum(earlier * expert_hot, axis=1)
    slot = flat_route * capacity + rank
    pick_hot = (slot[:, None] == jnp.arange(experts * capacity, dtype=jnp.int32)[None, :]).astype(
        jnp.bfloat16
    )
    row_hot = jnp.sum(pick_hot.reshape(own_rows, picks_row, experts * capacity), axis=1)
    outgoing = jnp.einsum("rs,rd->sd", row_hot, normed, preferred_element_type=jnp.float32).astype(
        jnp.bfloat16
    )
    outgoing = outgoing.reshape(experts, capacity, width)
    gate_local = gate_weight[0]
    up_local = up_weight[0]
    down_local = down_weight[0]
    arrived = lax.all_to_all(outgoing, "ep", split_axis=0, concat_axis=0, tiled=True)
    sources = arrived.shape[0]
    items = arrived.shape[1]
    slot_rows = arrived.reshape(sources * items, width)
    piece = collect(slot_rows, "tp", 0)
    gate = jnp.dot(piece, gate_local, preferred_element_type=jnp.float32)
    upper = jnp.dot(piece, up_local, preferred_element_type=jnp.float32)
    hidden = (jax.nn.silu(gate) * upper).astype(jnp.bfloat16)
    summed = sum_at_owner(
        jnp.dot(hidden, down_local, preferred_element_type=jnp.float32).astype(jnp.bfloat16),
        "tp",
        0,
    )
    worked = summed.astype(jnp.bfloat16).reshape(sources, items, width)
    mixer_out = sum_at_owner(
        jnp.dot(attended, out_weight, preferred_element_type=jnp.float32).astype(jnp.bfloat16),
        "tp",
        0,
    ).astype(jnp.bfloat16)
    back = lax.all_to_all(worked, "ep", split_axis=0, concat_axis=0, tiled=True)
    copies = jnp.dot(
        pick_hot, back.reshape(experts * capacity, width), preferred_element_type=jnp.float32
    )
    weighted = route_weight[..., None] * copies.reshape(own_rows, picks_row, width)
    mixed = jnp.sum(weighted, axis=1).astype(jnp.bfloat16)
    return (mixer_out, mixed)


def solution(mesh):
    placed = (
        P("ep", "tp"),
        P("ep", "tp"),
        P("ep", "tp"),
        P(),
        P(),
        P("tp", None),
        P(("ep", "tp"), None),
        P(),
        P(("ep", "tp"), None),
        P(("ep", "tp"), None),
        P("ep", None, "tp"),
        P("ep", None, "tp"),
        P("ep", "tp", None),
    )
    return jax.shard_map(
        local,
        mesh=mesh,
        in_specs=placed,
        out_specs=(P(("ep", "tp"), None), P(("ep", "tp"), None)),
        check_vma=False,
    )
```

profile of v0, /device:TPU:1, one launch (start us, length us, event | category | flops | bytes accessed | tf_op | source)
XLA Modules:
  0.0 269.1 jit_solution(2286914140994390860)
XLA Ops:
  9.4 1.4 pad_maximum_fusion.1
  14.0 1.3 convolution_convert_fusion.1
  15.6 31.5 %all_to_all.25 = bf16[64,2,2048]{2,1,0:T(2,128)(2,1)S(1)} all-to-all(bf16[64,2,2048]{2,1,0:T(2,128)(2,1)S(1)} %reshape.436), channel_id=1, replica_groups=mesh['ep'=64,'tp'=4] {'ep'}, dimensions={0} | all-to-all | bytes 1048576 | tf_op jit(solution)/shard_map/all_to_all | solution.py:156
  47.6 30.4 %all_to_all.26 = bf16[4,128,2048]{2,1,0:T(8,128)(2,1)S(1)} all-to-all(bf16[4,128,2048]{2,1,0:T(8,128)(2,1)S(1)} %broadcast_in_dim.11), channel_id=1, replica_groups=mesh['ep'=64,'tp'=4] {'tp'}, dimensions={0} | all-to-all | bytes 4194304 | tf_op jit(solution)/shard_map/all_to_all | solution.py:21
  78.0 3.6 %fusion.20 = f32[512,896]{1,0:T(8,128)} fusion(bf16[512,2048]{1,0:T(8,128)(2,1)S(1)} %bitcast.126, bf16[1,2048,896]{2,1,0:T(8,128)(2,1)S(1)} %copy-done.5), kind=kOutput, calls=%fused_computation.25 | convolution fusion | flops 1879048192 | bytes 7602176 | tf_op jit(solution)/shard_map/dot_general | solution.py:161
  81.5 9.6 %fusion.22 = bf16[512,2048]{1,0:T(8,128)(2,1)} fusion(bf16[1,896,2048]{2,1,0:T(8,128)(2,1)} %param.27, f32[512,896]{1,0:T(8,128)} %fusion.20, bf16[512,2048]{1,0:T(8,128)(2,1)S(1)} %bitcast.127, bf16[1,2048,896]{2,1,0:T(8,128)(2,1)} %param.26), kind=kOutput, calls=%fused_computation.27 | convolution fusion | flops 3761897472 | bytes 13369344 | tf_op jit(solution)/shard_map/dot_general | solution.py:165
  91.2 4.6 %all-to-all-start.3 = ((bf16[4,128,2048]{2,1,0:T(8,128)(2,1)}), bf16[4,128,2048]{2,1,0:T(8,128)(2,1)}, u32[]{:S(2)}, u32[]{:S(2)}) async-start(bf16[4,128,2048]{2,1,0:T(8,128)(2,1)} %bitcast.12), calls=%async_computation.3 | async-start | bytes 4194304 | tf_op jit(solution)/shard_map/all_to_all | solution.py:35
  97.3 23.6 %all-to-all-done.3 = bf16[4,128,2048]{2,1,0:T(8,128)(2,1)} async-done(((bf16[4,128,2048]{2,1,0:T(8,128)(2,1)}), bf16[4,128,2048]{2,1,0:T(8,128)(2,1)}, u32[]{:S(2)}, u32[]{:S(2)}) %all-to-all-start.3) | async-done | bytes 2097184 | tf_op jit(solution)/shard_map/all_to_all | solution.py:35
  120.9 2.0 reduce_sum.101
  122.9 1.2 reshape.440
  124.1 7.1 %all-to-all-start.4 = ((bf16[64,2,2048]{2,1,0:T(2,128)(2,1)}), bf16[64,2,2048]{2,1,0:T(2,128)(2,1)S(1)}, u32[]{:S(2)}, u32[]{:S(2)}) async-start(bf16[64,2,2048]{2,1,0:T(2,128)(2,1)} %reshape.440), calls=%async_computation.4 | async-start | bytes 1048576 | tf_op jit(solution)/shard_map/all_to_all | solution.py:175
  131.2 6.4 %copy.67 = bf16[16384,128]{1,0:T(8,128)(2,1)} copy(bf16[16384,128]{0,1:T(8,128)(2,1)} %all-gather.2.cloned.1.call-done) | data formatting | bytes 8388608 | tf_op jit(solution)/shard_map/all_gather | solution.py:116
  137.6 104.2 %while.15 = (s32[]{:T(128)}, f32[256,1,4]{0,2,1:T(4,128)S(1)}, f32[256,1,4]{0,2,1:T(4,128)S(1)}, f32[256,1,4,64]{0,3,2,1:T(8,128)S(1)}, bf16[8,2048,128]{2,1,0:T...) while((s32[]{:T(128)}, f32[256,1,4]{0,2,1:T(4,128)S(1)}, ...), condition=%wide.region_5.6_spmd.clone, body=%wide.region_2.5_spmd.clone.sunk | while | flops 553850880 | bytes 62062720 | solution.py:122
  137.6 1.1 constant_dynamic-slice_fusion.2
  138.9 4.5 %bitcast_reduce_fusion.3 = (f32[256,4]{0,1:T(4,128)S(1)}, f32[2048,256,4]{1,0,2:T(8,128)}) fusion(bf16[256,1,4,64]{0,3,2,1:T(8,128)(2,1)S(1)} %get-tuple-element.186, bf16[2048,128]{0,1:T(8,128)(2,1)S(1)} %bitcast.121), kind=kOutput, calls=%fused_computation.1.clone.1 | convolution fusion | flops 272628736 | bytes 8785920 | tf_op jit(solution)/shard_map/while/body/eval_jaxpr/qkgd,skd->qkgs/dot_general | solution.py:97
  143.4 5.1 %fusion.68 = f32[256,1,4,64]{0,3,2,1:T(8,128)S(1)} fusion(f32[2048,256,4]{1,0,2:T(8,128)} %get-tuple-element.163, f32[256,4]{0,1:T(4,128)S(1)} %bitcast.124, bf16[2048,128]{0,1:T(8,128)(2,1)S(1)} %bitcast.122, f32[256,1,4,64]{0,3,2,1:T(8,128)S(1)} %get-tuple-element.176, f32[256,4]{0,1:T(4,128)S(1)} %get-tuple-element.164, pred[]{:T(512)S(6)} %compare.14), kind=kOutput, calls=%fused_computation.8.clone.1 | convolution fusion | flops 274923520 | bytes 9183233 | tf_op jit(solution)/shard_map/while/body/eval_jaxpr/qkgs,skd->qkgd/dot_general | solution.py:104
  149.2 1.4 fusion.67
  150.6 1.1 constant_dynamic-slice_fusion.2
  151.9 4.5 %bitcast_reduce_fusion.3 = (f32[256,4]{0,1:T(4,128)S(1)}, f32[2048,256,4]{1,0,2:T(8,128)}) fusion(bf16[256,1,4,64]{0,3,2,1:T(8,128)(2,1)S(1)} %get-tuple-element.186, bf16[2048,128]{0,1:T(8,128)(2,1)S(1)} %bitcast.121), kind=kOutput, calls=%fused_computation.1.clone.1 | convolution fusion | flops 272628736 | bytes 8785920 | tf_op jit(solution)/shard_map/while/body/eval_jaxpr/qkgd,skd->qkgs/dot_general | solution.py:97
  156.4 5.1 %fusion.68 = f32[256,1,4,64]{0,3,2,1:T(8,128)S(1)} fusion(f32[2048,256,4]{1,0,2:T(8,128)} %get-tuple-element.163, f32[256,4]{0,1:T(4,128)S(1)} %bitcast.124, bf16[2048,128]{0,1:T(8,128)(2,1)S(1)} %bitcast.122, f32[256,1,4,64]{0,3,2,1:T(8,128)S(1)} %get-tuple-element.176, f32[256,4]{0,1:T(4,128)S(1)} %get-tuple-element.164, pred[]{:T(512)S(6)} %compare.14), kind=kOutput, calls=%fused_computation.8.clone.1 | convolution fusion | flops 274923520 | bytes 9183233 | tf_op jit(solution)/shard_map/while/body/eval_jaxpr/qkgs,skd->qkgd/dot_general | solution.py:104
  162.2 1.4 fusion.67
  163.6 1.1 constant_dynamic-slice_fusion.2
  164.9 4.5 %bitcast_reduce_fusion.3 = (f32[256,4]{0,1:T(4,128)S(1)}, f32[2048,256,4]{1,0,2:T(8,128)}) fusion(bf16[256,1,4,64]{0,3,2,1:T(8,128)(2,1)S(1)} %get-tuple-element.186, bf16[2048,128]{0,1:T(8,128)(2,1)S(1)} %bitcast.121), kind=kOutput, calls=%fused_computation.1.clone.1 | convolution fusion | flops 272628736 | bytes 8785920 | tf_op jit(solution)/shard_map/while/body/eval_jaxpr/qkgd,skd->qkgs/dot_general | solution.py:97
  169.5 5.1 %fusion.68 = f32[256,1,4,64]{0,3,2,1:T(8,128)S(1)} fusion(f32[2048,256,4]{1,0,2:T(8,128)} %get-tuple-element.163, f32[256,4]{0,1:T(4,128)S(1)} %bitcast.124, bf16[2048,128]{0,1:T(8,128)(2,1)S(1)} %bitcast.122, f32[256,1,4,64]{0,3,2,1:T(8,128)S(1)} %get-tuple-element.176, f32[256,4]{0,1:T(4,128)S(1)} %get-tuple-element.164, pred[]{:T(512)S(6)} %compare.14), kind=kOutput, calls=%fused_computation.8.clone.1 | convolution fusion | flops 274923520 | bytes 9183233 | tf_op jit(solution)/shard_map/while/body/eval_jaxpr/qkgs,skd->qkgd/dot_general | solution.py:104
  175.2 1.4 fusion.67
  176.7 1.1 constant_dynamic-slice_fusion.2
  178.0 4.5 %bitcast_reduce_fusion.3 = (f32[256,4]{0,1:T(4,128)S(1)}, f32[2048,256,4]{1,0,2:T(8,128)}) fusion(bf16[256,1,4,64]{0,3,2,1:T(8,128)(2,1)S(1)} %get-tuple-element.186, bf16[2048,128]{0,1:T(8,128)(2,1)S(1)} %bitcast.121), kind=kOutput, calls=%fused_computation.1.clone.1 | convolution fusion | flops 272628736 | bytes 8785920 | tf_op jit(solution)/shard_map/while/body/eval_jaxpr/qkgd,skd->qkgs/dot_general | solution.py:97
  182.5 5.1 %fusion.68 = f32[256,1,4,64]{0,3,2,1:T(8,128)S(1)} fusion(f32[2048,256,4]{1,0,2:T(8,128)} %get-tuple-element.163, f32[256,4]{0,1:T(4,128)S(1)} %bitcast.124, bf16[2048,128]{0,1:T(8,128)(2,1)S(1)} %bitcast.122, f32[256,1,4,64]{0,3,2,1:T(8,128)S(1)} %get-tuple-element.176, f32[256,4]{0,1:T(4,128)S(1)} %get-tuple-element.164, pred[]{:T(512)S(6)} %compare.14), kind=kOutput, calls=%fused_computation.8.clone.1 | convolution fusion | flops 274923520 | bytes 9183233 | tf_op jit(solution)/shard_map/while/body/eval_jaxpr/qkgs,skd->qkgd/dot_general | solution.py:104
  188.3 1.4 fusion.67
  189.7 1.1 constant_dynamic-slice_fusion.2
  191.0 4.5 %bitcast_reduce_fusion.3 = (f32[256,4]{0,1:T(4,128)S(1)}, f32[2048,256,4]{1,0,2:T(8,128)}) fusion(bf16[256,1,4,64]{0,3,2,1:T(8,128)(2,1)S(1)} %get-tuple-element.186, bf16[2048,128]{0,1:T(8,128)(2,1)S(1)} %bitcast.121), kind=kOutput, calls=%fused_computation.1.clone.1 | convolution fusion | flops 272628736 | bytes 8785920 | tf_op jit(solution)/shard_map/while/body/eval_jaxpr/qkgd,skd->qkgs/dot_general | solution.py:97
  195.5 5.1 %fusion.68 = f32[256,1,4,64]{0,3,2,1:T(8,128)S(1)} fusion(f32[2048,256,4]{1,0,2:T(8,128)} %get-tuple-element.163, f32[256,4]{0,1:T(4,128)S(1)} %bitcast.124, bf16[2048,128]{0,1:T(8,128)(2,1)S(1)} %bitcast.122, f32[256,1,4,64]{0,3,2,1:T(8,128)S(1)} %get-tuple-element.176, f32[256,4]{0,1:T(4,128)S(1)} %get-tuple-element.164, pred[]{:T(512)S(6)} %compare.14), kind=kOutput, calls=%fused_computation.8.clone.1 | convolution fusion | flops 274923520 | bytes 9183233 | tf_op jit(solution)/shard_map/while/body/eval_jaxpr/qkgs,skd->qkgd/dot_general | solution.py:104
  201.3 1.4 fusion.67
  202.7 1.1 constant_dynamic-slice_fusion.2
  204.0 4.5 %bitcast_reduce_fusion.3 = (f32[256,4]{0,1:T(4,128)S(1)}, f32[2048,256,4]{1,0,2:T(8,128)}) fusion(bf16[256,1,4,64]{0,3,2,1:T(8,128)(2,1)S(1)} %get-tuple-element.186, bf16[2048,128]{0,1:T(8,128)(2,1)S(1)} %bitcast.121), kind=kOutput, calls=%fused_computation.1.clone.1 | convolution fusion | flops 272628736 | bytes 8785920 | tf_op jit(solution)/shard_map/while/body/eval_jaxpr/qkgd,skd->qkgs/dot_general | solution.py:97
  208.5 5.1 %fusion.68 = f32[256,1,4,64]{0,3,2,1:T(8,128)S(1)} fusion(f32[2048,256,4]{1,0,2:T(8,128)} %get-tuple-element.163, f32[256,4]{0,1:T(4,128)S(1)} %bitcast.124, bf16[2048,128]{0,1:T(8,128)(2,1)S(1)} %bitcast.122, f32[256,1,4,64]{0,3,2,1:T(8,128)S(1)} %get-tuple-element.176, f32[256,4]{0,1:T(4,128)S(1)} %get-tuple-element.164, pred[]{:T(512)S(6)} %compare.14), kind=kOutput, calls=%fused_computation.8.clone.1 | convolution fusion | flops 274923520 | bytes 9183233 | tf_op jit(solution)/shard_map/while/body/eval_jaxpr/qkgs,skd->qkgd/dot_general | solution.py:104
  214.3 1.4 fusion.67
  215.7 1.1 constant_dynamic-slice_fusion.2
  217.0 4.5 %bitcast_reduce_fusion.3 = (f32[256,4]{0,1:T(4,128)S(1)}, f32[2048,256,4]{1,0,2:T(8,128)}) fusion(bf16[256,1,4,64]{0,3,2,1:T(8,128)(2,1)S(1)} %get-tuple-element.186, bf16[2048,128]{0,1:T(8,128)(2,1)S(1)} %bitcast.121), kind=kOutput, calls=%fused_computation.1.clone.1 | convolution fusion | flops 272628736 | bytes 8785920 | tf_op jit(solution)/shard_map/while/body/eval_jaxpr/qkgd,skd->qkgs/dot_general | solution.py:97
  221.6 5.1 %fusion.68 = f32[256,1,4,64]{0,3,2,1:T(8,128)S(1)} fusion(f32[2048,256,4]{1,0,2:T(8,128)} %get-tuple-element.163, f32[256,4]{0,1:T(4,128)S(1)} %bitcast.124, bf16[2048,128]{0,1:T(8,128)(2,1)S(1)} %bitcast.122, f32[256,1,4,64]{0,3,2,1:T(8,128)S(1)} %get-tuple-element.176, f32[256,4]{0,1:T(4,128)S(1)} %get-tuple-element.164, pred[]{:T(512)S(6)} %compare.14), kind=kOutput, calls=%fused_computation.8.clone.1 | convolution fusion | flops 274923520 | bytes 9183233 | tf_op jit(solution)/shard_map/while/body/eval_jaxpr/qkgs,skd->qkgd/dot_general | solution.py:104
  227.3 1.4 fusion.67
  228.8 1.1 constant_dynamic-slice_fusion.2
  230.1 4.5 %bitcast_reduce_fusion.3 = (f32[256,4]{0,1:T(4,128)S(1)}, f32[2048,256,4]{1,0,2:T(8,128)}) fusion(bf16[256,1,4,64]{0,3,2,1:T(8,128)(2,1)S(1)} %get-tuple-element.186, bf16[2048,128]{0,1:T(8,128)(2,1)S(1)} %bitcast.121), kind=kOutput, calls=%fused_computation.1.clone.1 | convolution fusion | flops 272628736 | bytes 8785920 | tf_op jit(solution)/shard_map/while/body/eval_jaxpr/qkgd,skd->qkgs/dot_general | solution.py:97
  234.6 5.1 %fusion.68 = f32[256,1,4,64]{0,3,2,1:T(8,128)S(1)} fusion(f32[2048,256,4]{1,0,2:T(8,128)} %get-tuple-element.163, f32[256,4]{0,1:T(4,128)S(1)} %bitcast.124, bf16[2048,128]{0,1:T(8,128)(2,1)S(1)} %bitcast.122, f32[256,1,4,64]{0,3,2,1:T(8,128)S(1)} %get-tuple-element.176, f32[256,4]{0,1:T(4,128)S(1)} %get-tuple-element.164, pred[]{:T(512)S(6)} %compare.14), kind=kOutput, calls=%fused_computation.8.clone.1 | convolution fusion | flops 274923520 | bytes 9183233 | tf_op jit(solution)/shard_map/while/body/eval_jaxpr/qkgs,skd->qkgd/dot_general | solution.py:104
  240.4 1.4 fusion.67
  241.8 1.5 convolution_convert_fusion
  243.3 3.5 %all-to-all-start = ((bf16[4,64,2048]{2,1,0:T(8,128)(2,1)}), bf16[4,64,2048]{2,1,0:T(8,128)(2,1)S(1)}, u32[]{:S(2)}, u32[]{:S(2)}) async-start(bf16[4,64,2048]{2,1,0:T(8,128)(2,1)} %bitcast.6), calls=%async_computation | async-start | bytes 2097152 | tf_op jit(solution)/shard_map/all_to_all | solution.py:35
  248.0 13.4 %all-to-all-done = bf16[4,64,2048]{2,1,0:T(8,128)(2,1)S(1)} async-done(((bf16[4,64,2048]{2,1,0:T(8,128)(2,1)}), bf16[4,64,2048]{2,1,0:T(8,128)(2,1)S(1)}, u32[]{:S(2)}, u32[]{:S(2)}) %all-to-all-start) | async-done | bytes 1048608 | tf_op jit(solution)/shard_map/all_to_all | solution.py:35
  (105 shorter events, 16.8 us)
Async XLA Ops:
  7.2 234.7 %copy-start = (bf16[256,2048]{1,0:T(8,128)(2,1)S(1)}, bf16[256,2048]{1,0:T(8,128)(2,1)}, u32[]{:S(2)}) copy-start(bf16[256,2048]{1,0:T(8,128)(2,1)} %param.20) | copy-start | bytes 3145732
  7.2 124.0 %all-gather.2.cloned.1.call-start = ((), (), s32[]{:S(2)}) async-start(), calls=%async_computation.5 | async-start | bytes 4259840 | tf_op jit(solution)/shard_map/all_gather | solution.py:116
  47.3 30.6 %copy-start.5 = (bf16[1,2048,896]{2,1,0:T(8,128)(2,1)S(1)}, bf16[1,2048,896]{2,1,0:T(8,128)(2,1)}, u32[]{:S(2)}) copy-start(bf16[1,2048,896]{2,1,0:T(8,128)(2,1)} %param.25) | copy-start | bytes 11010052
  91.2 4.6 %copy-start.2 = (bf16[256,256]{1,0:T(8,128)(2,1)S(1)}, bf16[256,256]{1,0:T(8,128)(2,1)}, u32[]{:S(2)}) copy-start(bf16[256,256]{1,0:T(8,128)(2,1)} %param.15) | copy-start | bytes 393220
  91.2 4.9 %copy-start.4 = (f32[64]{0:T(128)S(1)}, f32[64]{0:T(128)}, u32[]{:S(2)}) copy-start(f32[64]{0:T(128)} %param.18) | copy-start | bytes 772
  91.2 29.7 %all-to-all-start.3 = ((bf16[4,128,2048]{2,1,0:T(8,128)(2,1)}), bf16[4,128,2048]{2,1,0:T(8,128)(2,1)}, u32[]{:S(2)}, u32[]{:S(2)}) async-start(bf16[4,128,2048]{2,1,0:T(8,128)(2,1)} %bitcast.12), calls=%async_computation.3 | async-start | bytes 4194304 | tf_op jit(solution)/shard_map/all_to_all | solution.py:35
  124.1 119.2 %all-to-all-start.4 = ((bf16[64,2,2048]{2,1,0:T(2,128)(2,1)}), bf16[64,2,2048]{2,1,0:T(2,128)(2,1)S(1)}, u32[]{:S(2)}, u32[]{:S(2)}) async-start(bf16[64,2,2048]{2,1,0:T(2,128)(2,1)} %reshape.440), calls=%async_computation.4 | async-start | bytes 1048576 | tf_op jit(solution)/shard_map/all_to_all | solution.py:175
  143.4 5.8 %copy-start.1 = (f32[2048,256,4]{1,0,2:T(8,128)S(1)}, f32[2048,256,4]{1,0,2:T(8,128)}, u32[]{:S(2)}) copy-start(f32[2048,256,4]{1,0,2:T(8,128)} %get-tuple-element.163) | copy-start | bytes 25165828 | tf_op jit(solution)/shard_map/while
  156.4 5.8 %copy-start.1 = (f32[2048,256,4]{1,0,2:T(8,128)S(1)}, f32[2048,256,4]{1,0,2:T(8,128)}, u32[]{:S(2)}) copy-start(f32[2048,256,4]{1,0,2:T(8,128)} %get-tuple-element.163) | copy-start | bytes 25165828 | tf_op jit(solution)/shard_map/while
  169.5 5.8 %copy-start.1 = (f32[2048,256,4]{1,0,2:T(8,128)S(1)}, f32[2048,256,4]{1,0,2:T(8,128)}, u32[]{:S(2)}) copy-start(f32[2048,256,4]{1,0,2:T(8,128)} %get-tuple-element.163) | copy-start | bytes 25165828 | tf_op jit(solution)/shard_map/while
  182.5 5.8 %copy-start.1 = (f32[2048,256,4]{1,0,2:T(8,128)S(1)}, f32[2048,256,4]{1,0,2:T(8,128)}, u32[]{:S(2)}) copy-start(f32[2048,256,4]{1,0,2:T(8,128)} %get-tuple-element.163) | copy-start | bytes 25165828 | tf_op jit(solution)/shard_map/while
  195.5 5.8 %copy-start.1 = (f32[2048,256,4]{1,0,2:T(8,128)S(1)}, f32[2048,256,4]{1,0,2:T(8,128)}, u32[]{:S(2)}) copy-start(f32[2048,256,4]{1,0,2:T(8,128)} %get-tuple-element.163) | copy-start | bytes 25165828 | tf_op jit(solution)/shard_map/while
  208.5 5.8 %copy-start.1 = (f32[2048,256,4]{1,0,2:T(8,128)S(1)}, f32[2048,256,4]{1,0,2:T(8,128)}, u32[]{:S(2)}) copy-start(f32[2048,256,4]{1,0,2:T(8,128)} %get-tuple-element.163) | copy-start | bytes 25165828 | tf_op jit(solution)/shard_map/while
  221.6 5.8 %copy-start.1 = (f32[2048,256,4]{1,0,2:T(8,128)S(1)}, f32[2048,256,4]{1,0,2:T(8,128)}, u32[]{:S(2)}) copy-start(f32[2048,256,4]{1,0,2:T(8,128)} %get-tuple-element.163) | copy-start | bytes 25165828 | tf_op jit(solution)/shard_map/while
  234.6 5.8 %copy-start.1 = (f32[2048,256,4]{1,0,2:T(8,128)S(1)}, f32[2048,256,4]{1,0,2:T(8,128)}, u32[]{:S(2)}) copy-start(f32[2048,256,4]{1,0,2:T(8,128)} %get-tuple-element.163) | copy-start | bytes 25165828 | tf_op jit(solution)/shard_map/while
  241.8 5.2 %copy-start.3 = (f32[32,2]{0,1:T(2,128)S(1)}, f32[32,2]{0,1:T(2,128)}, u32[]{:S(2)}) copy-start(f32[32,2]{0,1:T(2,128)} %param.24) | copy-start | bytes 772
  243.3 18.1 %all-to-all-start = ((bf16[4,64,2048]{2,1,0:T(8,128)(2,1)}), bf16[4,64,2048]{2,1,0:T(8,128)(2,1)S(1)}, u32[]{:S(2)}, u32[]{:S(2)}) async-start(bf16[4,64,2048]{2,1,0:T(8,128)(2,1)} %bitcast.6), calls=%async_computation | async-start | bytes 2097152 | tf_op jit(solution)/shard_map/all_to_all | solution.py:35
Sparse Core Ops, SparseCore 0:
  11.2 83.0 all-gather.1
where the time goes:
time: 270 us; the launch traced here: 269 us
  matrix products  93.8 us (35%)
  blocking collectives  61.9 us (23%)
  waiting for transfers between devices  37.1 us (14%)
  local copies, waits for them, and re-layouts  25.7 us (10%)
  other arithmetic  20.8 us (8%)
  starting transfers between devices  15.2 us (6%)
  between operations  14.3 us (5%)
    dot_general x8, matrix products, fold_block(): jnp.einsum('qkgs,skd->qkgd', expo.astype(jnp.bfloat16), value_block, pref...  40.9 us
    all_to_all x2, waiting for transfers between devices, sum_at_owner(): lax.all_to_all(blocks, axis, split_axis=0, concat_axis=0, tiled=True)  37 us
    dot_general x8, matrix products, fold_block(): jnp.einsum('qkgd,skd->qkgs', rot_q, key_block, preferred_element_type=jnp...  36.1 us
    all_to_all x1, blocking collectives, local(): lax.all_to_all(outgoing, 'ep', split_axis=0, concat_axis=0, tiled=True)  31.5 us
    all_to_all x1, blocking collectives, copy_for_each(): return lax.all_to_all(copies, axis, split_axis=0, concat_axis=0, tiled=True)  30.4 us
    reduce_sum x8, other arithmetic, fold_block(): denom = denom * shrink + jnp.sum(expo, axis=-1)  11.1 us
    dynamic_slice x16, local copies, waits for them, and re-layouts, local(): carry, _ = lax.scan(fold_block, carry, blocks)  10.4 us
    dot_general x1, matrix products, local(): jnp.dot(hidden, down_local, preferred_element_type=jnp.float32)  9.65 us
  transfers between devices with their start and end apart: 4, of which 2 were waited for; matrix products, arithmetic and copies ran while one was open for 49% of the time, Pallas kernels for 0%

commit v1 on v0

v1 whole, which is shorter than its diff:
```python
import functools

import jax
import jax.numpy as jnp
from jax import lax
from jax.experimental import pallas as pl
from jax.experimental.pallas import tpu as pltpu
from jax.sharding import PartitionSpec as P

GRID_W = 64
EPS = 1e-06
THETA = 10000.0

NZ, NX = 8, 4
PLANES = (0, 7, 1, 6, 2, 5, 3, 4)
BF = jnp.bfloat16
F32 = jnp.float32
MESH = pl.DeviceIdType.MESH
RIGHT, OPP, LEFT = 1, 2, 3
F0, F1, D0, D1, E0, E1, S0, S1 = range(8)


def head_norm(vals, gain):
    vals = vals.astype(F32)
    return vals * lax.rsqrt(jnp.mean(vals * vals, axis=-1, keepdims=True) + EPS) * gain


def rotate(vals, positions):
    pairs = vals.shape[-1] // 2
    quarter = pairs // 2
    freqs = THETA ** (-jnp.arange(quarter, dtype=F32) / quarter)
    grid_row = (positions // GRID_W).astype(F32)
    grid_col = (positions % GRID_W).astype(F32)
    angle = jnp.concatenate([grid_row[:, None] * freqs, grid_col[:, None] * freqs], axis=-1)
    cosine = jnp.cos(angle)[:, None, :]
    sine = jnp.sin(angle)[:, None, :]
    split = vals.reshape(vals.shape[:-1] + (pairs, 2))
    first = split[..., 0]
    second = split[..., 1]
    turned = jnp.stack([first * cosine - second * sine, first * sine + second * cosine], axis=-1)
    return turned.reshape(vals.shape)


def body(
    q_ref,
    kvin_ref,
    outg_ref,
    gate_hbm,
    up_hbm,
    down_hbm,
    ow_hbm,
    mix_ref,
    back_ref,
    kv,
    xs,
    xm,
    hid,
    part,
    rsb,
    ret,
    att,
    m_s,
    acc,
    gate_v,
    up_v,
    down_v,
    ow_v,
    ssem,
    rsem,
    lsem,
):
    e = lax.axis_index("ep")
    t = lax.axis_index("tp")
    z, x, c = e // 8, lax.rem(e // 2, NX), lax.rem(e, 2)

    def dev(dz, dx, dc, dt=0):
        zz = lax.rem(z + (dz + NZ), NZ)
        xx = lax.rem(x + (dx + NX), NX)
        cc = c if dc == 0 else 1 - c
        tt = t if dt == 0 else lax.rem(t + (dt + 4), 4)
        return (zz * 8 + xx * 2 + cc, tt)

    used = [0]

    def sems():
        used[0] += 1
        return used[0] - 1

    def copy(src, dst, device, i=None):
        i = sems() if i is None else i
        return pltpu.make_async_remote_copy(
            src_ref=src,
            dst_ref=dst,
            send_sem=ssem.at[i],
            recv_sem=rsem.at[i],
            device_id=device,
            device_id_type=MESH,
        )

    kx = {
        3: copy(kvin_ref, kv.at[0, 0, 3], dev(0, 1, 0)),
        1: copy(kvin_ref, kv.at[0, 0, 1], dev(0, -1, 0)),
        2: copy(kvin_ref, kv.at[0, 0, 2], dev(0, 2, 0)),
    }
    kp0 = copy(kvin_ref, kv.at[0, 1, 0], dev(0, 0, 1))
    kpx = copy(kv.at[0, 0, pl.ds(1, 3)], kv.at[0, 1, pl.ds(1, 3)], dev(0, 0, 1))
    up_dev, down_dev, partner = dev(1, 0, 0), dev(-1, 0, 0), dev(0, 0, 1)
    hop_up = [copy(kv.at[(8 - i) % 8, 0], kv.at[7 - i, 0], up_dev) for i in range(3)]
    hop_down = [copy(kv.at[i, 0], kv.at[i + 1, 0], down_dev) for i in range(3)]
    hop_up.append(copy(kv.at[5, 0, pl.ds(0, 2)], kv.at[4, 0, pl.ds(0, 2)], up_dev))
    hop_down.append(copy(kv.at[3, 0, pl.ds(2, 2)], kv.at[4, 0, pl.ds(2, 2)], down_dev))
    pz = {d: copy(kv.at[d, 0], kv.at[d, 1], partner) for d in range(1, NZ)}

    spots = [
        (p, dx, dc) for p in range(NZ) for dx in range(NX) for dc in range(2)
    ]
    dsp_i, ret_i = [sems(), sems()], [sems(), sems()]
    dispatch, returns = [[], []], [[], []]
    for k, (p, dx, dc) in enumerate(spots):
        if k == 0:
            continue
        ch, j = k // 32, k % 32
        dz = PLANES[p]
        dispatch[ch].append(copy(outg_ref.at[k], xs.at[ch, 0, j], dev(-dz, -dx, dc), dsp_i[ch]))
        returns[ch].append(copy(ret.at[ch, j], back_ref.at[k], dev(dz, dx, dc), ret_i[ch]))

    def span(ref, ch):
        return ref.at[pl.ds(1, 31)] if ch == 0 else ref.at[pl.ds(0, 32)]

    def dispatch_all(ch):
        view = span(xs.at[ch, 0], ch)
        return copy(view, view, partner, dsp_i[ch])

    def return_all(ch):
        view = back_ref.at[pl.ds(1, 31)] if ch == 0 else back_ref.at[pl.ds(32, 32)]
        return copy(view, view, partner, ret_i[ch])

    right, left = dev(0, 0, 0, 1), dev(0, 0, 0, -1)
    lo, hi = pl.ds(0, 16), pl.ds(16, 16)
    ag = []
    for ch in range(2):
        ag.append(
            (
                copy(xs.at[ch, 0, lo], xs.at[ch, LEFT, lo], right),
                copy(xs.at[ch, 0, hi], xs.at[ch, RIGHT, hi], left),
                copy(xs.at[ch, 0, hi], xs.at[ch, LEFT, hi], right),
                copy(xs.at[ch, 0, lo], xs.at[ch, RIGHT, lo], left),
                copy(xs.at[ch, LEFT, lo], xs.at[ch, OPP, lo], right),
                copy(xs.at[ch, RIGHT, hi], xs.at[ch, OPP, hi], left),
            )
        )
    lo, hi = pl.ds(0, 32), pl.ds(32, 32)
    rs = []
    for i in range(3):
        pi, bi = part.at[i], rsb.at[i]
        rs.append(
            (
                copy(pi.at[OPP, lo], bi.at[F0], right),
                copy(pi.at[OPP, hi], bi.at[F1], left),
                copy(pi.at[RIGHT, hi], bi.at[D1], right),
                copy(pi.at[LEFT, lo], bi.at[D0], left),
                copy(bi.at[S0], bi.at[E0], right),
                copy(bi.at[S1], bi.at[E1], left),
            )
        )

    loads = [
        pltpu.make_async_copy(src, dst, lsem.at[i])
        for i, (src, dst) in enumerate(
            [(gate_hbm, gate_v), (up_hbm, up_v), (down_hbm, down_v), (ow_hbm, ow_v)]
        )
    ]

    def gather_first(ch):
        dispatch_all(ch).wait_recv()
        for one in ag[ch][:4]:
            one.start()

    def gather_second(ch):
        ag[ch][0].wait_recv()
        ag[ch][4].start()
        ag[ch][1].wait_recv()
        ag[ch][5].start()

    def reduce_first(i):
        for one in rs[i][:4]:
            one.start()

    def reduce_second(i):
        for copied, slot, other, half, sent, way in (
            (0, F0, RIGHT, 0, S0, 4),
            (1, F1, LEFT, 32, S1, 5),
        ):
            rs[i][copied].wait_recv()
            for r in range(2):
                rows = pl.ds(16 * r, 16)
                own = part[i, other, pl.ds(half + 16 * r, 16)].astype(F32)
                rsb[i, sent, rows] = (rsb[i, slot, rows].astype(F32) + own).astype(BF)
            rs[i][way].start()

    def reduce_last(i, store):
        for direct, passed, d, pe, half in ((3, 4, D0, E0, 0), (2, 5, D1, E1, 32)):
            rs[i][direct].wait_recv()
            rs[i][passed].wait_recv()
            for r in range(2):
                rows = pl.ds(16 * r, 16)
                total = (
                    part[i, 0, pl.ds(half + 16 * r, 16)].astype(F32)
                    + rsb[i, d, rows].astype(F32)
                    + rsb[i, pe, rows].astype(F32)
                ).astype(BF)
                store(half + 16 * r, total)

    def experts(ch):
        for n in (2, 3, 4, 5):
            ag[ch][n].wait_recv()
        if ch == 0:
            for one in loads[:3]:
                one.wait()

        def relay(g, _):
            r, q = g // 4, lax.rem(g, 4)
            rows = xs[ch, r, pl.ds(q * 8, 8)].reshape(16, 2048)
            xm[pl.ds(pl.multiple_of(g * 16, 16), 16), :] = rows
            return 0

        lax.fori_loop(0, 16, relay, 0)

        def widen(n, _):
            cols = pl.ds(pl.multiple_of(n * 128, 128), 128)
            both = jnp.concatenate([gate_v[:, cols], up_v[:, cols]], axis=1)
            made = jnp.dot(xm[...], both, preferred_element_type=F32)
            gate, upper = made[:, :128], made[:, 128:]
            hid[:, cols] = (gate / (1.0 + jnp.exp(-gate)) * upper).astype(BF)
            return 0

        lax.fori_loop(0, 7, widen, 0)

        def narrow(n, _):
            cols = pl.ds(pl.multiple_of(n * 256, 256), 256)
            made = jnp.dot(hid[...], down_v[:, cols], preferred_element_type=F32).astype(BF)
            for r in range(4):
                part[ch, r, :, cols] = made[r * 64 : (r + 1) * 64]
            return 0

        lax.fori_loop(0, 8, narrow, 0)
        reduce_first(ch)

    def give_back(ch):
        def store(row, total):
            ret[ch, pl.ds(row // 2, 8)] = total.reshape(8, 2, 2048)

        reduce_last(ch, store)
        if ch == 0:
            back_ref[0] = ret[0, 0]
        for one in returns[ch]:
            one.start()

    barrier = pltpu.get_barrier_semaphore()
    for k, (p, dx, dc) in enumerate(spots):
        if k:
            pl.semaphore_signal(
                barrier, inc=1, device_id=dev(PLANES[p], dx, dc), device_id_type=MESH
            )
    for peer in (right, left):
        pl.semaphore_signal(barrier, inc=1, device_id=peer, device_id_type=MESH)
    for one in loads:
        one.start()
    kv[0, 0, 0] = kvin_ref[...]
    xs[0, 0, 0] = outg_ref[0]
    m_s[...] = jnp.full_like(m_s, -1e30)
    acc[...] = jnp.zeros_like(acc)
    pl.semaphore_wait(barrier, 65)

    kp0.start()
    for one in kx.values():
        one.start()
    for ch in range(2):
        for one in dispatch[ch]:
            one.start()
    for one in kx.values():
        one.wait_recv()
    kpx.start()
    hop_up[0].start()
    hop_down[0].start()
    gather_first(0)
    kp0.wait_recv()
    kpx.wait_recv()

    def pass_on(i):
        hop_up[i].wait_recv()
        hop_down[i].wait_recv()
        if i < 3:
            hop_up[i + 1].start()
            hop_down[i + 1].start()
            pz[7 - i].start()
            pz[i + 1].start()
        else:
            pz[4].start()

    def at1():
        gather_second(0)
        gather_first(1)
        experts(0)
        gather_second(1)
        pass_on(0)
        pz[7].wait_recv()

    def at2():
        reduce_second(0)
        pz[1].wait_recv()

    def at3():
        experts(1)
        pass_on(1)
        give_back(0)
        pz[6].wait_recv()

    def at4():
        reduce_second(1)
        pz[2].wait_recv()

    def at5():
        pass_on(2)
        give_back(1)
        pz[5].wait_recv()

    def at6():
        pz[3].wait_recv()

    def at7():
        pass_on(3)
        pz[4].wait_recv()

    events = {1: at1, 2: at2, 3: at3, 4: at4, 5: at5, 6: at6, 7: at7}

    def step(s, _):
        for at, event in events.items():
            pl.when(s == at)(event)
        odd = lax.rem(s, 2)
        dz = odd * (8 - (s + 1) // 2) + (1 - odd) * (s // 2)
        keyed = kv[dz].reshape(2048, 128)
        lane = lax.broadcasted_iota(jnp.int32, keyed.shape, 1)
        valued = jnp.where(lane == 0, jnp.ones_like(keyed), keyed)

        def score(h):
            return lax.dot_general(
                q_ref[pl.ds(h * 256, 256), :],
                keyed,
                (((1,), (1,)), ((), ())),
                preferred_element_type=F32,
            )

        highs = [m_s[h] for h in range(4)]
        sums = [acc[h] for h in range(4)]
        new_high, new_sum = [], []
        ahead = score(0)
        for h in range(4):
            now = ahead
            if h < 3:
                ahead = score(h + 1)
            high = jnp.maximum(highs[h], jnp.max(now, axis=1, keepdims=True))
            probs = jnp.exp(now - high).astype(BF)
            made = jnp.dot(probs, valued, preferred_element_type=F32)
            new_sum.append(sums[h] * jnp.exp(highs[h] - high) + made)
            new_high.append(high)
        for h in range(4):
            m_s[h] = new_high[h]
            acc[h] = new_sum[h]
        return 0

    lax.fori_loop(0, 8, step, 0)

    for pair in range(2):
        both = []
        for h in (2 * pair, 2 * pair + 1):
            total = acc[h]
            both.append((total / total[:, 0:1])[:, 64:].astype(BF))
        att[:, pair * 128 : (pair + 1) * 128] = jnp.concatenate(both, axis=1)
    loads[3].wait()

    def project(n, _):
        cols = pl.ds(pl.multiple_of(n * 256, 256), 256)
        made = jnp.dot(att[...], ow_v[:, cols], preferred_element_type=F32).astype(BF)
        for b in range(4):
            part[2, lax.rem(b + 4 - t, 4), :, cols] = made[b * 64 : (b + 1) * 64]
        return 0

    lax.fori_loop(0, 8, project, 0)
    reduce_first(2)
    reduce_second(2)

    def store_mix(row, total):
        mix_ref[pl.ds(row, 16), :] = total

    reduce_last(2, store_mix)
    for ch in range(2):
        return_all(ch).wait_recv()
    for one in [*kx.values(), kp0, kpx, *hop_up, *hop_down, *pz.values()]:
        one.wait_send()
    for ch in range(2):
        dispatch_all(ch).wait_send()
        return_all(ch).wait_send()
        for one in ag[ch]:
            one.wait_send()
    for i in range(3):
        for one in rs[i]:
            one.wait_send()


def local(
    queries,
    keys,
    values,
    q_gain,
    k_gain,
    out_weight,
    tokens,
    ffn_gain,
    route,
    route_weight,
    gate_weight,
    up_weight,
    down_weight,
):
    e = lax.axis_index("ep")
    z, x, c = e // 8, (e // 2) % 4, e % 2
    positions = e * 256 + jnp.arange(256, dtype=jnp.int32)
    rot_q = rotate(head_norm(queries.reshape(256, 4, 64), q_gain), positions).astype(BF)
    rot_q = rot_q * jnp.asarray(0.125, BF)
    rot_q = jnp.pad(jnp.moveaxis(rot_q, 1, 0), ((0, 0), (0, 0), (0, 64))).reshape(1024, 128)
    rot_k = rotate(head_norm(keys.reshape(256, 1, 64), k_gain), positions).astype(BF)
    joined = jnp.concatenate([rot_k.reshape(256, 64), values], axis=1)

    token_float = tokens.astype(F32)
    normed = (
        token_float
        * lax.rsqrt(jnp.mean(token_float * token_float, axis=-1, keepdims=True) + EPS)
        * ffn_gain
    ).astype(BF)
    spot = jnp.arange(64, dtype=jnp.int32)
    place = spot // 8
    dz = jnp.where(place % 2 == 1, 8 - (place + 1) // 2, place // 2)
    dx, dc = (spot // 2) % 4, spot % 2
    target = ((z - dz) % 8) * 8 + ((x - dx) % 4) * 2 + (c + dc) % 2
    flat_route = route.reshape(-1)
    hot = (flat_route[:, None] == target[None, :]).astype(BF)
    before = (jnp.arange(64)[:, None] > jnp.arange(64)[None, :]).astype(BF)
    earlier = jnp.dot(before, hot, preferred_element_type=F32)
    rank = jnp.sum(earlier * hot.astype(F32), axis=1)
    ranked = (rank[:, None] == jnp.arange(2, dtype=F32)[None, :]).astype(BF)
    pick_hot = (hot[:, :, None] * ranked[:, None, :]).reshape(64, 128)
    row_hot = jnp.sum(pick_hot.reshape(32, 2, 128), axis=1)
    outgoing = jnp.einsum("rs,rd->sd", row_hot, normed, preferred_element_type=F32).astype(BF)
    outgoing = outgoing.reshape(64, 2, 2048)

    vmem = pl.BlockSpec(memory_space=pltpu.VMEM)
    hbm = pl.BlockSpec(memory_space=pl.ANY)
    mixer_out, back = pl.pallas_call(
        body,
        out_shape=(
            jax.ShapeDtypeStruct((64, 2048), BF),
            jax.ShapeDtypeStruct((64, 2, 2048), BF),
        ),
        in_specs=[vmem] * 3 + [hbm] * 4,
        out_specs=(vmem, vmem),
        scratch_shapes=[
            pltpu.VMEM((8, 2, 4, 256, 128), BF),
            pltpu.VMEM((2, 4, 32, 2, 2048), BF),
            pltpu.VMEM((256, 2048), BF),
            pltpu.VMEM((256, 896), BF),
            pltpu.VMEM((3, 4, 64, 2048), BF),
            pltpu.VMEM((3, 8, 32, 2048), BF),
            pltpu.VMEM((2, 32, 2, 2048), BF),
            pltpu.VMEM((256, 256), BF),
            pltpu.VMEM((4, 256, 1), F32),
            pltpu.VMEM((4, 256, 128), F32),
            pltpu.VMEM((2048, 896), BF),
            pltpu.VMEM((2048, 896), BF),
            pltpu.VMEM((896, 2048), BF),
            pltpu.VMEM((256, 2048), BF),
            pltpu.SemaphoreType.DMA((64,)),
            pltpu.SemaphoreType.DMA((64,)),
            pltpu.SemaphoreType.DMA((4,)),
        ],
        compiler_params=pltpu.CompilerParams(
            collective_id=0, has_side_effects=True, vmem_limit_bytes=60 << 20
        ),
        name="fused",
    )(
        rot_q,
        joined,
        outgoing,
        gate_weight[0],
        up_weight[0],
        down_weight[0],
        out_weight,
    )
    copies = jnp.dot(pick_hot, back.reshape(128, 2048), preferred_element_type=F32)
    weighted = route_weight[..., None] * copies.reshape(32, 2, 2048)
    mixed = jnp.sum(weighted, axis=1).astype(BF)
    return (mixer_out, mixed)


def solution(mesh):
    placed = (
        P("ep", "tp"),
        P("ep", "tp"),
        P("ep", "tp"),
        P(),
        P(),
        P("tp", None),
        P(("ep", "tp"), None),
        P(),
        P(("ep", "tp"), None),
        P(("ep", "tp"), None),
        P("ep", None, "tp"),
        P("ep", None, "tp"),
        P("ep", "tp", None),
    )
    return jax.shard_map(
        local,
        mesh=mesh,
        in_specs=placed,
        out_specs=(P(("ep", "tp"), None), P(("ep", "tp"), None)),
        check_vma=False,
    )
```

time: 270 us -> 113 us (0.42)
  Pallas kernels: 0 us -> 94.1 us
  matrix products: 93.8 us -> 1.44 us
  blocking collectives: 61.9 us -> 0 us
  waiting for transfers between devices: 37.1 us -> 0 us
  other arithmetic: 20.8 us -> 5.56 us
  starting transfers between devices: 15.2 us -> 0 us
  local copies, waits for them, and re-layouts: 25.7 us -> 10.7 us
  between operations: 14.3 us -> 0.89 us
    pallas_call x0 -> x1, Pallas kernels: none -> 94.1 us  [local(): pl.pallas_call(body, out_shape=(jax.ShapeDtypeStruct((64, 2048), BF), jax...]
    dot_general x21 -> x3, matrix products: 93.8 us -> 1.44 us  [the longest x1 0.88 us: local(): jnp.dot(pick_hot, back.reshape(128, 2048), preferred_element_type=F32)]
    all_to_all x2 -> x0, blocking collectives: 61.9 us -> none  [the longest x1 31.5 us: local(): lax.all_to_all(outgoing, 'ep', split_axis=0, concat_axis=0, tiled=True)]
    all_to_all x3 -> x0, waiting for transfers between devices: 37 us -> none  [the longest x2 37 us: sum_at_owner(): lax.all_to_all(blocks, axis, split_axis=0, concat_axis=0, tiled=True)]
    all_to_all x3 -> x0, starting transfers between devices: 15.2 us -> none  [the longest x2 8.11 us: sum_at_owner(): lax.all_to_all(blocks, axis, split_axis=0, concat_axis=0, tiled=True)]
    reduce_sum x12 -> x1, other arithmetic: 14.3 us -> 0.05 us  [local(): row_hot = jnp.sum(pick_hot.reshape(32, 2, 128), axis=1)]
    dynamic_slice x16 -> x0, local copies, waits for them, and re-layouts: 10.4 us -> none  [local(): carry, _ = lax.scan(fold_block, carry, blocks)]
    all_gather x1 -> x0, local copies, waits for them, and re-layouts: 6.36 us -> none  [local(): piece = lax.all_gather(joined, 'ep', axis=0, tiled=True)]
  transfers between devices with their start and end apart: 4 -> 0, of which waited for: 2 -> 0; matrix products, arithmetic and copies ran while one was open for 49% -> 0% of each run, Pallas kernels for 0% -> 0%
where the time goes in v1:
time: 113 us
  Pallas kernels  94.1 us (83%)
  local copies, waits for them, and re-layouts  10.7 us (9%)
  other arithmetic  5.56 us (5%)
  matrix products  1.44 us (1%)
    pallas_call x1, Pallas kernels, local(): pl.pallas_call(body, out_shape=(jax.ShapeDtypeStruct((64, 2048), BF), jax...  94.1 us
    unnamed x11, local copies, waits for them, and re-layouts  4.53 us

profile of v1, /device:TPU:1, one launch (start us, length us, event | category | flops | bytes accessed | tf_op | source)
XLA Modules:
  0.0 112.7 jit_solution(7137919969762078569)
XLA Ops:
  0.7 0.0 copy-start
  0.7 0.0 copy-start.1
  0.7 1.1 fusion.2
  1.8 0.8 fusion.8
  2.6 0.8 mul.255
  3.4 0.8 copy.48
  4.2 0.1 eq.56
  4.3 0.2 fusion.1
  4.5 0.1 compare_convert_fusion
  4.6 0.1 copy.49
  4.7 0.1 fusion.11
  4.7 0.1 fusion.19
  4.8 0.8 fusion.9
  5.7 0.1 fusion.34
  5.8 0.1 subtract_convert_fusion.1
  6.0 0.1 copy.46
  6.1 0.9 copy.47
  7.0 0.7 pad_maximum_fusion.kvin_ref
  7.7 0.1 fusion.15
  7.8 1.0 copy.40
  8.9 0.1 reshape.533
  9.1 0.2 multiply_multiply_fusion
  9.3 0.3 subtract_convert_fusion
  9.6 0.3 maximum_multiply_fusion
  9.9 0.1 copy.41
  10.0 0.2 copy.53
  10.2 0.8 pad.4.clone
  11.0 0.6 broadcast_multiply_fusion
  11.6 1.6 %mul.288 = bf16[32,2,128]{2,1,0:T(2,128)(2,1)S(1)} reshape(bf16[64,64,2]{2,1,0:T(8,128)(2,1)S(1)} %broadcast_multiply_fusion) | data formatting | bytes 32768 | tf_op jit(solution)/shard_map/mul | solution.py:452
  13.2 0.1 reduce_sum.60
  13.2 0.0 copy-done
  13.3 0.0 copy-done.1
  13.3 0.3 convolution_convert_fusion
  13.6 1.1 %reshape.531.outg_ref = bf16[64,2,2048]{2,1,0:T(2,128)(2,1)} reshape(bf16[128,2048]{1,0:T(8,128)(2,1)S(1)} %convolution_convert_fusion) | data formatting | bytes 1048576 | tf_op jit(solution)/shard_map/reshape | solution.py:455
  14.7 0.0 copy-start.2
  14.7 94.1 %fused.1 = (bf16[64,2048]{1,0:T(8,128)(2,1)}, bf16[64,2,2048]{2,1,0:T(2,128)(2,1)}) custom-call(bf16[1024,128]{1,0:T(8,128)(2,1)} %bitcast.24, bf16[256,128]{1,0:T(8,128)(2,1)} %pad_maximum_fusion.kvin_ref, bf16[64,2,2048]{2,1,0:T(2,128)(2,1)} %reshape.531.outg_ref, bf16[2048,896]{1,0:T(8,128)(2,1)} %bitcast.21, bf16[2048,896]{1,0:T(8,128)(2,1)} %bitcast.22, ...), custom_call_target="tpu_custom_call" | custom-call | tf_op jit(solution)/shard_map/fused/pallas_call | solution.py:459
  108.9 1.2 %reshape.534 = bf16[128,2048,1]{1,0,2:T(8,128)(2,1)S(1)} reshape(bf16[64,2,2048]{2,1,0:T(2,128)(2,1)} %get-tuple-element.5) | data formatting | bytes 1048576 | tf_op jit(solution)/shard_map/reshape | solution.py:499
  110.1 0.0 copy-done.2
  110.1 0.9 fusion
  111.0 1.7 %copy.61 = bf16[64,2048]{1,0:T(8,128)(2,1)} copy(bf16[64,2048]{1,0:T(8,128)(2,1)} %get-tuple-element.24) | data formatting | bytes 524288
  (11 shorter events, 0.2 us)
Async XLA Ops:
  0.7 12.6 %copy-start = (bf16[32,2048]{1,0:T(8,128)(2,1)S(1)}, bf16[32,2048]{1,0:T(8,128)(2,1)}, u32[]{:S(2)}) copy-start(bf16[32,2048]{1,0:T(8,128)(2,1)} %param.19) | copy-start | bytes 393220
  0.7 12.6 %copy-start.1 = (f32[2048]{0:T(1024)S(1)}, f32[2048]{0:T(1024)}, u32[]{:S(2)}) copy-start(f32[2048]{0:T(1024)} %param.20) | copy-start | bytes 24580
  14.7 95.4 %copy-start.2 = (f32[32,2]{0,1:T(2,128)S(1)}, f32[32,2]{0,1:T(2,128)}, u32[]{:S(2)}) copy-start(f32[32,2]{0,1:T(2,128)} %param.22) | copy-start | bytes 772

commit v2 on v1

v2 whole, which is shorter than its diff:
```python
import jax
import jax.numpy as jnp
import numpy as np
from jax import lax
from jax.experimental import pallas as pl
from jax.experimental.pallas import tpu as pltpu
from jax.sharding import PartitionSpec as P

EPS = 1e-06
THETA = 10000.0

NZ, NX = 8, 4
PLANES = (0, 7, 1, 4, 6, 2, 5, 3)
BF = jnp.bfloat16
F32 = jnp.float32
MESH = pl.DeviceIdType.MESH
RIGHT, OPP, LEFT = 1, 2, 3
F0, F1, D0, D1, E0, E1, S0, S1 = range(8)


def body(
    queries_hbm,
    keys_hbm,
    values_hbm,
    tokens_hbm,
    gate_hbm,
    up_hbm,
    down_hbm,
    ow_hbm,
    q_gain,
    k_gain,
    ffn_gain,
    freqs,
    route,
    weight,
    mix_ref,
    mixed_ref,
    kv,
    xs,
    xm,
    hid,
    part,
    rsb,
    ret,
    back_ref,
    outg_ref,
    picks,
    att,
    q_ref,
    m_s,
    acc,
    gate_v,
    up_v,
    down_v,
    ow_v,
    queries,
    keys,
    values,
    tokens,
    ssem,
    rsem,
    lsem,
):
    e = lax.axis_index("ep")
    t = lax.axis_index("tp")
    z, x, c = e // 8, lax.rem(e // 2, NX), lax.rem(e, 2)

    def dev(dz, dx, dc, dt=0):
        zz = lax.rem(z + (dz + NZ), NZ)
        xx = lax.rem(x + (dx + NX), NX)
        cc = c if dc == 0 else 1 - c
        tt = t if dt == 0 else lax.rem(t + (dt + 4), 4)
        return (zz * 8 + xx * 2 + cc, tt)

    used = [0]

    def sems():
        used[0] += 1
        return used[0] - 1

    def copy(src, dst, device, i=None):
        i = sems() if i is None else i
        return pltpu.make_async_remote_copy(
            src_ref=src,
            dst_ref=dst,
            send_sem=ssem.at[i],
            recv_sem=rsem.at[i],
            device_id=device,
            device_id_type=MESH,
        )

    up_dev, down_dev, partner = dev(1, 0, 0), dev(-1, 0, 0), dev(0, 0, 1)
    near, far = dev(0, 1, 0), dev(0, -1, 0)
    top, low = pl.ds(0, 128), pl.ds(128, 128)
    hop_up = [copy(kv.at[(8 - i) % 8, 0, 0], kv.at[7 - i, 0, 0], up_dev) for i in range(3)]
    hop_down = [copy(kv.at[i, 0, 0], kv.at[i + 1, 0, 0], down_dev) for i in range(3)]
    hop_up.append(copy(kv.at[5, 0, 0, top], kv.at[4, 0, 0, top], up_dev))
    hop_down.append(copy(kv.at[3, 0, 0, low], kv.at[4, 0, 0, low], down_dev))
    x_near = [copy(kv.at[d, 0, 0], kv.at[d, 0, 3], near) for d in range(NZ)]
    x_far = [copy(kv.at[d, 0, 0], kv.at[d, 0, 1], far) for d in range(NZ)]
    x_near2 = {d: copy(kv.at[d, 0, 3, top], kv.at[d, 0, 2, top], near) for d in range(1, NZ)}
    x_far2 = {d: copy(kv.at[d, 0, 1, low], kv.at[d, 0, 2, low], far) for d in range(1, NZ)}
    across = [copy(kv.at[d, 0], kv.at[d, 1], partner) for d in range(NZ)]
    x_two = copy(kv.at[0, 0, 0], kv.at[0, 0, 2], dev(0, 2, 0))

    spots = [
        (p, dx, dc) for p in range(NZ) for dx in range(NX) for dc in range(2)
    ]
    dsp_i, ret_i = [sems(), sems()], [sems(), sems()]
    dispatch, returns = [[], []], [[], []]
    for k, (p, dx, dc) in enumerate(spots):
        if k == 0:
            continue
        ch, j = k // 32, k % 32
        dz = PLANES[p]
        dispatch[ch].append(copy(outg_ref.at[k], xs.at[ch, 0, j], dev(-dz, -dx, dc), dsp_i[ch]))
        returns[ch].append(copy(ret.at[ch, j], back_ref.at[k], dev(dz, dx, dc), ret_i[ch]))

    def dispatch_all(ch):
        view = xs.at[ch, 0, pl.ds(1, 31)] if ch == 0 else xs.at[ch, 0]
        return copy(view, view, partner, dsp_i[ch])

    def return_all(ch):
        view = back_ref.at[pl.ds(1, 31)] if ch == 0 else back_ref.at[pl.ds(32, 32)]
        return copy(view, view, partner, ret_i[ch])

    right, left = dev(0, 0, 0, 1), dev(0, 0, 0, -1)
    lo, hi = pl.ds(0, 16), pl.ds(16, 16)
    ag = []
    for ch in range(2):
        ag.append(
            (
                copy(xs.at[ch, 0, lo], xs.at[ch, LEFT, lo], right),
                copy(xs.at[ch, 0, hi], xs.at[ch, RIGHT, hi], left),
                copy(xs.at[ch, 0, hi], xs.at[ch, LEFT, hi], right),
                copy(xs.at[ch, 0, lo], xs.at[ch, RIGHT, lo], left),
                copy(xs.at[ch, LEFT, lo], xs.at[ch, OPP, lo], right),
                copy(xs.at[ch, RIGHT, hi], xs.at[ch, OPP, hi], left),
            )
        )
    lo, hi = pl.ds(0, 32), pl.ds(32, 32)
    rs = []
    for i in range(3):
        pi, bi = part.at[i], rsb.at[i]
        rs.append(
            (
                copy(pi.at[OPP, lo], bi.at[F0], right),
                copy(pi.at[OPP, hi], bi.at[F1], left),
                copy(pi.at[RIGHT, hi], bi.at[D1], right),
                copy(pi.at[LEFT, lo], bi.at[D0], left),
                copy(bi.at[S0], bi.at[E0], right),
                copy(bi.at[S1], bi.at[E1], left),
            )
        )

    loads = [
        pltpu.make_async_copy(src, dst, lsem.at[i])
        for i, (src, dst) in enumerate(
            [
                (keys_hbm, keys),
                (values_hbm, values),
                (tokens_hbm, tokens),
                (queries_hbm, queries),
                (gate_hbm, gate_v),
                (up_hbm, up_v),
                (down_hbm, down_v),
                (ow_hbm, ow_v),
            ]
        )
    ]

    def gather_first(ch):
        dispatch_all(ch).wait_recv()
        for one in ag[ch][:4]:
            one.start()

    def gather_second(ch):
        ag[ch][0].wait_recv()
        ag[ch][4].start()
        ag[ch][1].wait_recv()
        ag[ch][5].start()

    def reduce_first(i):
        for one in rs[i][:4]:
            one.start()

    def reduce_middle(i, side):
        copied, slot, other, half, sent, way = (
            (0, F0, RIGHT, 0, S0, 4),
            (1, F1, LEFT, 32, S1, 5),
        )[side]
        rs[i][copied].wait_recv()
        for r in range(2):
            rows = pl.ds(16 * r, 16)
            own = part[i, other, pl.ds(half + 16 * r, 16)].astype(F32)
            rsb[i, sent, rows] = (rsb[i, slot, rows].astype(F32) + own).astype(BF)
        rs[i][way].start()

    def reduce_second(i):
        reduce_middle(i, 0)
        reduce_middle(i, 1)

    def reduce_last(i, store):
        for direct, passed, d, pe, half in ((3, 4, D0, E0, 0), (2, 5, D1, E1, 32)):
            rs[i][direct].wait_recv()
            rs[i][passed].wait_recv()
            for r in range(2):
                rows = pl.ds(16 * r, 16)
                total = (
                    part[i, 0, pl.ds(half + 16 * r, 16)].astype(F32)
                    + rsb[i, d, rows].astype(F32)
                    + rsb[i, pe, rows].astype(F32)
                ).astype(BF)
                store(half + 16 * r, total)

    def experts(ch, meanwhile):
        for n in (2, 3, 4, 5):
            ag[ch][n].wait_recv()
        if ch == 0:
            for one in loads[4:7]:
                one.wait()

        def relay(g, _):
            r, q = g // 4, lax.rem(g, 4)
            rows = xs[ch, r, pl.ds(q * 8, 8)].reshape(16, 2048)
            xm[pl.ds(pl.multiple_of(g * 16, 16), 16), :] = rows
            return 0

        lax.fori_loop(0, 16, relay, 0)

        def widen(n, _):
            cols = pl.ds(pl.multiple_of(n * 128, 128), 128)
            both = jnp.concatenate([gate_v[:, cols], up_v[:, cols]], axis=1)
            made = jnp.dot(xm[...], both, preferred_element_type=F32)
            gate, upper = made[:, :128], made[:, 128:]
            hid[:, cols] = (gate / (1.0 + jnp.exp(-gate)) * upper).astype(BF)
            return 0

        lax.fori_loop(0, 7, widen, 0, unroll=7)
        meanwhile()

        def narrow(n, _):
            cols = pl.ds(pl.multiple_of(n * 256, 256), 256)
            made = jnp.dot(hid[...], down_v[:, cols], preferred_element_type=F32).astype(BF)
            for r in range(4):
                part[ch, r, :, cols] = made[r * 64 : (r + 1) * 64]
            return 0

        lax.fori_loop(0, 8, narrow, 0, unroll=8)
        reduce_first(ch)

    def give_back(ch):
        def store(row, total):
            ret[ch, pl.ds(row // 2, 8)] = total.reshape(8, 2, 2048)

        reduce_last(ch, store)
        if ch == 0:
            back_ref[0] = ret[0, 0]
        for one in returns[ch]:
            one.start()

    barrier = pltpu.get_barrier_semaphore()
    for k, (p, dx, dc) in enumerate(spots):
        if k:
            pl.semaphore_signal(
                barrier, inc=1, device_id=dev(PLANES[p], dx, dc), device_id_type=MESH
            )
    for peer in (right, left):
        pl.semaphore_signal(barrier, inc=1, device_id=peer, device_id_type=MESH)
    for one in loads:
        one.start()

    lane = lax.broadcasted_iota(jnp.int32, (64, 128), 1)
    line = lax.broadcasted_iota(jnp.int32, (64, 128), 0)
    across_angle = line.astype(F32) * freqs[...]
    at_row = jnp.where(line[:8] < 4, line[:8], (line[:8] + t) & 3)
    down_angle = (at_row + e * 4).astype(F32) * freqs[...]
    even = (lane & 1) == 0
    by_row = (lane & 63) < 32
    first = lane < 64
    col_cos, col_sin = jnp.cos(across_angle), jnp.sin(across_angle)
    row_cos, row_sin = jnp.cos(down_angle), jnp.sin(down_angle)

    def turned(vals, gain, b):
        square = vals * vals
        one = jnp.sum(jnp.where(first, square, 0.0), axis=1, keepdims=True)
        two = jnp.sum(jnp.where(first, 0.0, square), axis=1, keepdims=True)
        mean = jnp.where(first, one, two) * (1.0 / 64)
        vals = vals * lax.rsqrt(mean + EPS) * gain
        swapped = jnp.where(even, pltpu.roll(vals, 127, 1), pltpu.roll(vals, 1, 1))
        cosine = jnp.where(by_row, row_cos[b : b + 1], col_cos)
        sine = jnp.where(by_row, row_sin[b : b + 1], col_sin)
        return vals * cosine + swapped * jnp.where(even, -sine, sine)

    loads[0].wait()
    loads[1].wait()
    gain = jnp.concatenate([k_gain[...], k_gain[...]], axis=1)
    for b in range(4):
        cols = pl.ds((b // 2) * 128, 128)
        half = slice((b % 2) * 64, (b % 2) * 64 + 64)
        key_rows = keys[:, cols].astype(F32).T[half]
        value_rows = values[:, cols].astype(F32).T[half]
        doubled = turned(jnp.concatenate([key_rows, key_rows], axis=1), gain, b)
        value_rows = jnp.concatenate([value_rows, value_rows], axis=1)
        kv[0, 0, 0, pl.ds(b * 64, 64), :] = jnp.where(first, doubled, value_rows).astype(BF)

    slot = lax.broadcasted_iota(jnp.int32, (128, 32), 0)
    spot, order = slot >> 1, (slot & 1).astype(F32)
    place = spot >> 3
    back_z = sum(jnp.where(place == p, dz, 0) for p, dz in enumerate(PLANES))
    target = (
        ((z + 8 - back_z) & 7) * 8
        + ((x + 4 - ((spot >> 1) & 3)) & 3) * 2
        + ((c + (spot & 1)) & 1)
    )
    named = [jnp.where(route[k : k + 1, :] == target, 1.0, 0.0) for k in range(2)]
    any_named = named[0] + named[1]
    rows_at = lax.broadcasted_iota(jnp.int32, (32, 32), 0)
    cols_at = lax.broadcasted_iota(jnp.int32, (32, 32), 1)
    before = jnp.where(rows_at < cols_at, 1.0, 0.0).astype(BF)
    rank = jnp.dot(any_named.astype(BF), before, preferred_element_type=F32)
    fits = jnp.where(rank == order, 1.0, 0.0)
    for k in range(2):
        picks[k] = (named[k] * fits).astype(BF)
    chosen = (any_named * fits).astype(BF)
    loads[2].wait()
    own = tokens[...].astype(F32)
    mean = jnp.mean(own * own, axis=1, keepdims=True)
    normed = (own * lax.rsqrt(mean + EPS) * ffn_gain[...]).astype(BF)
    for n in range(4):
        cols = slice(n * 512, n * 512 + 512)
        made = jnp.dot(chosen, normed[:, cols], preferred_element_type=F32)
        xm[0:128, cols] = made.astype(BF)

    def pack(g, _):
        rows = xm[pl.ds(pl.multiple_of(g * 16, 16), 16), :]
        outg_ref[pl.ds(g * 8, 8)] = rows.reshape(8, 2, 2048)
        return 0

    lax.fori_loop(0, 8, pack, 0)
    xs[0, 0, 0] = outg_ref[0]
    pl.semaphore_wait(barrier, 65)

    def send_rows(ch, planes):
        skip = 1 if ch == 0 else 0
        for p in planes:
            first_at = max(p * 8 - skip, 0)
            for one in dispatch[ch][first_at : p * 8 + 8 - skip]:
                one.start()

    def hops(d):
        if d:
            hop_up[d - 1].wait_recv()
            hop_down[d - 1].wait_recv()
        if d < 4:
            hop_up[d].start()
            hop_down[d].start()
        for at in {(8 - d) % 8, d}:
            x_near[at].start()
            x_far[at].start()

    def sides(d):
        for at in {(8 - d) % 8, d}:
            x_near[at].wait_recv()
            x_near2[at].start()
            x_far[at].wait_recv()
            x_far2[at].start()

    def cross(d):
        for at in {(8 - d) % 8, d}:
            x_near2[at].wait_recv()
            x_far2[at].wait_recv()
            across[at].start()

    hops(0)
    x_two.start()
    send_rows(0, range(4))
    loads[3].wait()
    gain = jnp.concatenate([q_gain[...], q_gain[...]], axis=1)
    for r in range(4):
        tokens_at = pl.ds(pl.multiple_of(lax.rem(t + r, 4) * 64, 64), 64)
        for pair in range(2):
            vals = queries[tokens_at, pair * 128 : pair * 128 + 128].astype(F32)
            done = turned(vals, gain, 4 + r).astype(BF).astype(F32) * 0.125
            rows = pl.ds(r * 256 + 2 * pair * 64, 64)
            q_ref[rows, :] = jnp.where(first, done, 0.0).astype(BF)
            rows = pl.ds(r * 256 + (2 * pair + 1) * 64, 64)
            q_ref[rows, :] = jnp.where(first, pltpu.roll(done, 64, 1), 0.0).astype(BF)
    m_s[...] = jnp.full_like(m_s, -1e30)
    acc[...] = jnp.zeros_like(acc)

    def at0():
        x_near[0].wait_recv()
        x_far[0].wait_recv()
        x_two.wait_recv()
        across[0].start()
        hops(1)
        send_rows(1, range(4))
        across[0].wait_recv()

    def in0():
        sides(1)
        gather_first(0)

    def at1():
        hops(2)
        cross(1)
        across[7].wait_recv()

    def in1():
        sides(2)
        hops(3)

    def at2():
        gather_second(0)
        gather_first(1)
        across[1].wait_recv()

    def in2():
        cross(2)
        sides(3)

    def at3():
        hops(4)
        experts(0, during0)
        across[6].wait_recv()

    def in3():
        cross(3)
        sides(4)

    def during0():
        gather_second(1)

    def during1():
        cross(4)
        reduce_second(0)

    def fold(high, total, scores, valued):
        above = jnp.maximum(high, jnp.max(scores, axis=1, keepdims=True))
        probs = jnp.exp(scores - above).astype(BF)
        made = jnp.dot(probs, valued, preferred_element_type=F32)
        return above, total * jnp.exp(high - above) + made

    def score(unit, keyed):
        return lax.dot_general(
            q_ref[pl.ds(pl.multiple_of(unit * 256, 256), 256), :],
            keyed,
            (((1,), (1,)), ((), ())),
            preferred_element_type=F32,
        )

    def with_ones(keyed):
        at = lax.broadcasted_iota(jnp.int32, keyed.shape, 1)
        return jnp.where(at == 0, jnp.ones_like(keyed), keyed)

    events = {0: at0, 1: at1, 2: at2, 3: at3}
    inside = {0: in0, 1: in1, 2: in2, 3: in3}

    def near_step(s, _):
        for at, event in events.items():
            pl.when(s == at)(event)
        odd = lax.rem(s, 2)
        dz = odd * (8 - (s + 1) // 2) + (1 - odd) * (s // 2)
        keyed = kv[dz].reshape(2048, 128)
        valued = with_ones(keyed)
        held = [(m_s[u], acc[u]) for u in range(4)]
        ahead = score(0, keyed)
        for u in range(4):
            now = ahead
            if u < 3:
                ahead = score(u + 1, keyed)
            m_s[u], acc[u] = fold(*held[u], now, valued)
            if u == 1:
                for at, event in inside.items():
                    pl.when(s == at)(event)
        return 0

    lax.fori_loop(0, 4, near_step, 0)

    experts(1, during1)
    for at in (2, 5, 3, 4):
        across[at].wait_recv()
    loads[7].wait()

    def between1():
        give_back(0)
        reduce_second(1)

    def between2():
        give_back(1)

    def far_step(s, _):
        for at, event in ((1, between1), (3, between2)):
            pl.when(s == at)(event)
        unit = lax.rem(2 + 3 * s + 3 * (s // 2) + 2 * (s // 3), 4)
        high, total = m_s[unit], acc[unit]
        blocks = [kv[dz].reshape(2048, 128) for dz in (2, 5, 3, 4)]
        ahead = score(unit, blocks[0])
        for i in range(4):
            now = ahead
            if i < 3:
                ahead = score(unit, blocks[i + 1])
            high, total = fold(high, total, now, with_ones(blocks[i]))
        scaled = (total / total[:, 0:1])[:, 64:].astype(BF)
        att[...] = jnp.concatenate([scaled[h * 64 : h * 64 + 64] for h in range(4)], axis=1)

        def project(n, _):
            cols = pl.ds(pl.multiple_of(n * 256, 256), 256)
            made = jnp.dot(att[...], ow_v[:, cols], preferred_element_type=F32)
            part[2, unit, :, cols] = made.astype(BF)
            return 0

        lax.fori_loop(0, 8, project, 0, unroll=8)

        @pl.when(s == 0)
        def _():
            rs[2][0].start()
            rs[2][1].start()

        @pl.when(s == 1)
        def _():
            rs[2][2].start()
            reduce_middle(2, 0)

        @pl.when(s == 2)
        def _():
            rs[2][3].start()
            reduce_middle(2, 1)

        return 0

    lax.fori_loop(0, 4, far_step, 0)

    def store_mix(row, total):
        mix_ref[pl.ds(row, 16), :] = total

    reduce_last(2, store_mix)
    for ch in range(2):
        return_all(ch).wait_recv()

    def unpack(g, _):
        rows = back_ref[pl.ds(g * 8, 8)].reshape(16, 2048)
        xm[pl.ds(pl.multiple_of(g * 16, 16), 16), :] = rows
        return 0

    lax.fori_loop(0, 8, unpack, 0)
    share = [
        jnp.sum(jnp.where(rows_at == cols_at, weight[k : k + 1, :], 0.0), axis=1, keepdims=True)
        for k in range(2)
    ]
    for n in range(4):
        cols = slice(n * 512, n * 512 + 512)
        came = [
            lax.dot_general(
                picks[k],
                xm[0:128, cols],
                (((0,), (0,)), ((), ())),
                preferred_element_type=F32,
            )
            for k in range(2)
        ]
        mixed_ref[:, cols] = (share[0] * came[0] + share[1] * came[1]).astype(BF)

    halves = [*x_near2.values(), *x_far2.values()]
    for one in [*hop_up, *hop_down, *x_near, *x_far, *halves, *across, x_two]:
        one.wait_send()
    for ch in range(2):
        dispatch_all(ch).wait_send()
        return_all(ch).wait_send()
        for one in ag[ch]:
            one.wait_send()
    for i in range(3):
        for one in rs[i]:
            one.wait_send()


def local(
    queries,
    keys,
    values,
    q_gain,
    k_gain,
    out_weight,
    tokens,
    ffn_gain,
    route,
    route_weight,
    gate_weight,
    up_weight,
    down_weight,
):
    pair = (np.arange(128) % 64) // 2
    freqs = np.power(THETA, -(pair % 16) / 16.0).astype(np.float32).reshape(1, 128)
    vmem = pl.BlockSpec(memory_space=pltpu.VMEM)
    hbm = pl.BlockSpec(memory_space=pl.ANY)
    return pl.pallas_call(
        body,
        out_shape=(
            jax.ShapeDtypeStruct((64, 2048), BF),
            jax.ShapeDtypeStruct((32, 2048), BF),
        ),
        in_specs=[hbm] * 8 + [vmem] * 6,
        out_specs=(vmem, vmem),
        scratch_shapes=[
            pltpu.VMEM((8, 2, 4, 256, 128), BF),
            pltpu.VMEM((2, 4, 32, 2, 2048), BF),
            pltpu.VMEM((256, 2048), BF),
            pltpu.VMEM((256, 896), BF),
            pltpu.VMEM((3, 4, 64, 2048), BF),
            pltpu.VMEM((3, 8, 32, 2048), BF),
            pltpu.VMEM((2, 32, 2, 2048), BF),
            pltpu.VMEM((64, 2, 2048), BF),
            pltpu.VMEM((64, 2, 2048), BF),
            pltpu.VMEM((2, 128, 32), BF),
            pltpu.VMEM((64, 256), BF),
            pltpu.VMEM((1024, 128), BF),
            pltpu.VMEM((4, 256, 1), F32),
            pltpu.VMEM((4, 256, 128), F32),
            pltpu.VMEM((2048, 896), BF),
            pltpu.VMEM((2048, 896), BF),
            pltpu.VMEM((896, 2048), BF),
            pltpu.VMEM((256, 2048), BF),
            pltpu.VMEM((256, 256), BF),
            pltpu.VMEM((64, 256), BF),
            pltpu.VMEM((64, 256), BF),
            pltpu.VMEM((32, 2048), BF),
            pltpu.SemaphoreType.DMA((96,)),
            pltpu.SemaphoreType.DMA((96,)),
            pltpu.SemaphoreType.DMA((8,)),
        ],
        compiler_params=pltpu.CompilerParams(
            collective_id=0, has_side_effects=True, vmem_limit_bytes=60 << 20
        ),
        name="fused",
    )(
        queries,
        keys.T,
        values.T,
        tokens,
        gate_weight[0],
        up_weight[0],
        down_weight[0],
        out_weight,
        q_gain.reshape(1, 64),
        k_gain.reshape(1, 64),
        ffn_gain.reshape(1, 2048),
        jnp.asarray(freqs),
        route.T,
        route_weight.T,
    )


def solution(mesh):
    placed = (
        P("ep", "tp"),
        P("ep", "tp"),
        P("ep", "tp"),
        P(),
        P(),
        P("tp", None),
        P(("ep", "tp"), None),
        P(),
        P(("ep", "tp"), None),
        P(("ep", "tp"), None),
        P("ep", None, "tp"),
        P("ep", None, "tp"),
        P("ep", "tp", None),
    )
    return jax.shard_map(
        local,
        mesh=mesh,
        in_specs=placed,
        out_specs=(P(("ep", "tp"), None), P(("ep", "tp"), None)),
        check_vma=False,
    )
```

time: 113 us -> 84.5 us (0.75)
  Pallas kernels: 94.1 us -> 79.5 us
  local copies, waits for them, and re-layouts: 10.7 us -> 3.24 us
  other arithmetic: 5.56 us -> 0 us
  matrix products: 1.44 us -> 0 us
    pallas_call x1, Pallas kernels: 94.1 us -> 79.5 us  [local(): pl.pallas_call(body, out_shape=(jax.ShapeDtypeStruct((64, 2048), BF), jax...]
    mul x3 -> x0, local copies, waits for them, and re-layouts: 2.43 us -> none  [the longest x1 1.57 us: local(): pick_hot = (hot[:, :, None] * ranked[:, None, :]).reshape(64, 128)]
    reshape x3 -> x0, local copies, waits for them, and re-layouts: 2.41 us -> none  [the longest x1 1.24 us: local(): back.reshape(128, 2048)]
    mul x4 -> x0, other arithmetic: 1.96 us -> none  [the longest x2 1.04 us: head_norm(): vals * lax.rsqrt(jnp.mean(vals * vals, axis=-1, keepdims=True) + EPS) * gain]
    reduce_sum x4 -> x0, other arithmetic: 1.95 us -> none  [the longest x1 1.07 us: local(): jnp.mean(token_float * token_float, axis=-1, keepdims=True) + EPS]
    dot_general x3 -> x0, matrix products: 1.44 us -> none  [the longest x1 0.88 us: local(): jnp.dot(pick_hot, back.reshape(128, 2048), preferred_element_type=F32)]
    unnamed x11 -> x2, local copies, waits for them, and re-layouts: 4.53 us -> 3.24 us
where the time goes in v2:
time: 84.5 us; the launch traced here: 83.4 us
  Pallas kernels  79.5 us (94%)
  local copies, waits for them, and re-layouts  3.24 us (4%)
    pallas_call x1, Pallas kernels, local(): pl.pallas_call(body, out_shape=(jax.ShapeDtypeStruct((64, 2048), BF), jax...  79.5 us
    unnamed x2, local copies, waits for them, and re-layouts  3.24 us

profile of v2, /device:TPU:1, one launch (start us, length us, event | category | flops | bytes accessed | tf_op | source)
XLA Modules:
  0.0 83.4 jit_solution(11228356872587556286)
XLA Ops:
  0.6 79.5 %fused.1 = (bf16[64,2048]{1,0:T(8,128)(2,1)}, bf16[32,2048]{1,0:T(8,128)(2,1)}) custom-call(bf16[256,256]{1,0:T(8,128)(2,1)} %queries_hbm.1, bf16[64,256]{1,0:T(8,128)(2,1)} %bitcast.13, bf16[64,256]{1,0:T(8,128)(2,1)} %bitcast.14, bf16[32,2048]{1,0:T(8,128)(2,1)} %tokens_hbm.1, bf16[2048,896]{1,0:T(8,128)(2,1)} %bitcast.10, bf16[2048,896]{1,0:T(8,128)(2,1)} %bitcast.11, ...), custom_call_target="tpu_custom_call" | custom-call | tf_op jit(solution)/shard_map/fused/pallas_call | solution.py:597
  80.2 1.7 %copy.18 = bf16[64,2048]{1,0:T(8,128)(2,1)} copy(bf16[64,2048]{1,0:T(8,128)(2,1)} %get-tuple-element.4) | data formatting | bytes 524288
  81.8 1.6 %copy.19 = bf16[32,2048]{1,0:T(8,128)(2,1)} copy(bf16[32,2048]{1,0:T(8,128)(2,1)} %get-tuple-element.5) | data formatting | bytes 262144

commit v3 on v2

--- a/solution.py
+++ b/solution.py
@@ -10,7 +10,7 @@
 THETA = 10000.0
 
 NZ, NX = 8, 4
-PLANES = (0, 7, 1, 4, 6, 2, 5, 3)
+PLANES = (0, 4, 1, 7, 5, 3, 6, 2)
 BF = jnp.bfloat16
 F32 = jnp.float32
 MESH = pl.DeviceIdType.MESH
@@ -399,29 +399,27 @@
         across[0].wait_recv()
 
     def in0():
+        gather_first(0)
         sides(1)
-        gather_first(0)
 
     def at1():
         hops(2)
         cross(1)
         across[7].wait_recv()
+        gather_second(0)
 
     def in1():
         sides(2)
         hops(3)
+        gather_first(1)
 
     def at2():
-        gather_second(0)
-        gather_first(1)
         across[1].wait_recv()
 
-    def in2():
+    def at3():
+        hops(4)
         cross(2)
         sides(3)
-
-    def at3():
-        hops(4)
         experts(0, during0)
         across[6].wait_recv()
 
@@ -455,7 +453,7 @@
         return jnp.where(at == 0, jnp.ones_like(keyed), keyed)
 
     events = {0: at0, 1: at1, 2: at2, 3: at3}
-    inside = {0: in0, 1: in1, 2: in2, 3: in3}
+    inside = {0: in0, 1: in1, 3: in3}
 
     def near_step(s, _):
         for at, event in events.items():
@@ -479,29 +477,35 @@
     lax.fori_loop(0, 4, near_step, 0)
 
     experts(1, during1)
-    for at in (2, 5, 3, 4):
+    for at in (2, 5, 3):
         across[at].wait_recv()
     loads[7].wait()
 
-    def between1():
-        give_back(0)
+    def mid1():
         reduce_second(1)
-
-    def between2():
+        rs[2][0].start()
+        rs[2][1].start()
+
+    def between3():
         give_back(1)
 
     def far_step(s, _):
-        for at, event in ((1, between1), (3, between2)):
-            pl.when(s == at)(event)
+        pl.when(s == 3)(between3)
         unit = lax.rem(2 + 3 * s + 3 * (s // 2) + 2 * (s // 3), 4)
         high, total = m_s[unit], acc[unit]
-        blocks = [kv[dz].reshape(2048, 128) for dz in (2, 5, 3, 4)]
-        ahead = score(unit, blocks[0])
+
+        def block(i):
+            return kv[(2, 5, 3, 4)[i]].reshape(2048, 128)
+
+        ahead = score(unit, block(0))
         for i in range(4):
             now = ahead
             if i < 3:
-                ahead = score(unit, blocks[i + 1])
-            high, total = fold(high, total, now, with_ones(blocks[i]))
+                ahead = score(unit, block(i + 1))
+            high, total = fold(high, total, now, with_ones(block(i)))
+            if i == 1:
+                pl.when(s == 0)(across[4].wait_recv)
+                pl.when(s == 1)(mid1)
         scaled = (total / total[:, 0:1])[:, 64:].astype(BF)
         att[...] = jnp.concatenate([scaled[h * 64 : h * 64 + 64] for h in range(4)], axis=1)
 
@@ -515,22 +519,21 @@
 
         @pl.when(s == 0)
         def _():
-            rs[2][0].start()
-            rs[2][1].start()
+            give_back(0)
 
         @pl.when(s == 1)
         def _():
             rs[2][2].start()
-            reduce_middle(2, 0)
 
         @pl.when(s == 2)
         def _():
             rs[2][3].start()
-            reduce_middle(2, 1)
 
         return 0
 
     lax.fori_loop(0, 4, far_step, 0)
+
+    reduce_second(2)
 
     def store_mix(row, total):
         mix_ref[pl.ds(row, 16), :] = total
@@ -573,6 +576,15 @@
     for i in range(3):
         for one in rs[i]:
             one.wait_send()
+
+
+def write(one_ref, two_ref, one_out, two_out, sem):
+    first = pltpu.make_async_copy(one_ref, one_out, sem.at[0])
+    second = pltpu.make_async_copy(two_ref, two_out, sem.at[1])
+    first.start()
+    second.start()
+    first.wait()
+    second.wait()
 
 
 def local(
@@ -594,7 +606,7 @@
     freqs = np.power(THETA, -(pair % 16) / 16.0).astype(np.float32).reshape(1, 128)
     vmem = pl.BlockSpec(memory_space=pltpu.VMEM)
     hbm = pl.BlockSpec(memory_space=pl.ANY)
-    return pl.pallas_call(
+    made = pl.pallas_call(
         body,
         out_shape=(
             jax.ShapeDtypeStruct((64, 2048), BF),
@@ -649,6 +661,17 @@
         route.T,
         route_weight.T,
     )
+    return pl.pallas_call(
+        write,
+        out_shape=(
+            jax.ShapeDtypeStruct((64, 2048), BF),
+            jax.ShapeDtypeStruct((32, 2048), BF),
+        ),
+        in_specs=[vmem] * 2,
+        out_specs=(hbm, hbm),
+        scratch_shapes=[pltpu.SemaphoreType.DMA((2,))],
+        name="write",
+    )(*made)
 
 
 def solution(mesh):

time: 84.5 us -> 78.4 us (0.928); the launches traced: 83.4 us -> 78.3 us
  local copies, waits for them, and re-layouts: 3.24 us -> 0 us
  Pallas kernels: 79.5 us -> 77.5 us
    pallas_call x1, Pallas kernels: 79.5 us -> 75.7 us  [local(): pl.pallas_call(body, out_shape=(jax.ShapeDtypeStruct((64, 2048), BF), jax...]
    unnamed x2 -> x0, local copies, waits for them, and re-layouts: 3.24 us -> none
    pallas_call x0 -> x1, Pallas kernels: none -> 1.74 us  [local(): pl.pallas_call(write, out_shape=(jax.ShapeDtypeStruct((64, 2048), BF), ja...]
where the time goes in v3:
time: 78.4 us; the launch traced here: 78.3 us
  Pallas kernels  77.5 us (99%)
  between operations  0.8 us (1%)
    pallas_call x1, Pallas kernels, local(): pl.pallas_call(body, out_shape=(jax.ShapeDtypeStruct((64, 2048), BF), jax...  75.7 us
    pallas_call x1, Pallas kernels, local(): pl.pallas_call(write, out_shape=(jax.ShapeDtypeStruct((64, 2048), BF), ja...  1.74 us

profile of v3, /device:TPU:1, one launch (start us, length us, event | category | flops | bytes accessed | tf_op | source)
XLA Modules:
  0.0 78.3 jit_solution(8427141819895349750)
XLA Ops:
  0.6 75.7 %fused.1 = (bf16[64,2048]{1,0:T(8,128)(2,1)}, bf16[32,2048]{1,0:T(8,128)(2,1)}) custom-call(bf16[256,256]{1,0:T(8,128)(2,1)} %queries_hbm.1, bf16[64,256]{1,0:T(8,128)(2,1)} %bitcast.13, bf16[64,256]{1,0:T(8,128)(2,1)} %bitcast.14, bf16[32,2048]{1,0:T(8,128)(2,1)} %tokens_hbm.1, bf16[2048,896]{1,0:T(8,128)(2,1)} %bitcast.10, bf16[2048,896]{1,0:T(8,128)(2,1)} %bitcast.11, ...), custom_call_target="tpu_custom_call" | custom-call | tf_op jit(solution)/shard_map/fused/pallas_call | solution.py:609
  76.4 1.7 %write.1 = (bf16[64,2048]{1,0:T(8,128)(2,1)}, bf16[32,2048]{1,0:T(8,128)(2,1)}) custom-call(bf16[64,2048]{1,0:T(8,128)(2,1)} %get-tuple-element.4.one_ref, bf16[32,2048]{1,0:T(8,128)(2,1)} %get-tuple-element.5.two_ref), custom_call_target="tpu_custom_call" | custom-call | tf_op jit(solution)/shard_map/write/pallas_call | solution.py:664
